TPU v7x, 32 devices: a whole 2x2x4 slice. The times are simulated.
32 devices in a mesh: sp: 4 (over z), dp: 8 (over y, x, core).
Axes of the slice: x: 2, y: 2, z: 4, core: 2. Of those that a mesh axis runs over, the one named last changes fastest.
Arguments:
- cotangent: bfloat16 [8, 512, 2048], P('dp', 'sp'), may hold values from -6 to 6
- unit_pre: bfloat16 [8, 512, 2048], P('dp', None, 'sp'), may hold values from -6 to 6
- gate_pre: bfloat16 [8, 512, 2048], P('dp', None, 'sp'), may hold values from -15 to 15
- out_weight: bfloat16 [2048, 2048], P('dp', 'sp'), may hold values from -0.125 to 0.125
- mix_weight: bfloat16 [8, 128, 128], replicated, may hold values from -0.5 to 0.5
- mix_bias: bfloat16 [8, 128], replicated, may hold values from 0.099609375 to 1.8984375
- norm_gain: bfloat16 [2048], P('sp'), may hold values from 0.099609375 to 1.8984375
- norm_shift: bfloat16 [2048], P('sp'), may hold values from -3 to 3
Outputs:
- unit_grad: bfloat16 [8, 512, 2048], P('dp', None, 'sp')
- gate_grad: bfloat16 [8, 512, 2048], P('dp', None, 'sp')
- out_weight_grad: float32 [2048, 2048], P('dp', 'sp')
- mix_weight_grad: float32 [8, 128, 128], replicated
- mix_bias_grad: float32 [8, 128], replicated
- gain_grad: float32 [2048], P('sp')
- shift_grad: float32 [2048], P('sp')
All inputs are finite; a program needn't handle non-finite values.
Results may differ from a plain program's by a relative error of at most 0.015.
Values may be sent and summed in bfloat16 or wider, within the bound.
No kernel may reach another device: no remote copies, remote signals or barrier semaphores. Data moves between devices by JAX's collectives and lax.ppermute only.
A program may use at most 64 MiB of HBM per device.

v0:
```python
import math
import jax
import jax.numpy as jnp
from jax import lax
from jax.sharding import PartitionSpec as P

GW = 2048
GROUPS = 8
BLK = 128
epsilon = 1e-05
tanh_coef = math.sqrt(2.0 / math.pi)


def gelu_slope(values):
    inner = tanh_coef * (values + 0.044715 * values * values * values)
    hyper = jnp.tanh(inner)
    return 0.5 * (1.0 + hyper) + 0.5 * values * (1.0 - hyper * hyper) * tanh_coef * (
        1.0 + 3.0 * 0.044715 * values * values
    )


def local(cotangent, unit_pre, gate_pre, out_weight, mix_weight, mix_bias, norm_gain, norm_shift):
    seq_len = unit_pre.shape[1]
    channels = unit_pre.shape[2]
    group_dim = GW // GROUPS
    span_width = min(channels, group_dim)
    groups_here = channels // span_width
    blocks = seq_len // BLK
    group_start = lax.axis_index("sp") * channels // group_dim
    units = unit_pre[0].astype(jnp.float32)
    gates = gate_pre[0].astype(jnp.float32)
    unit_act = jax.nn.gelu(units)
    gate_act = jax.nn.gelu(gates)
    moments = lax.psum((jnp.sum(gate_act, axis=-1), jnp.sum(gate_act * gate_act, axis=-1)), "sp")
    mean_val = moments[0] / GW
    var_val = moments[1] / GW - mean_val * mean_val
    rstd_val = lax.rsqrt(var_val + epsilon)
    centred = (gate_act - mean_val[:, None]) * rstd_val[:, None]
    gain_vec = norm_gain.astype(jnp.float32)
    normed = (centred * gain_vec + norm_shift.astype(jnp.float32)).astype(jnp.bfloat16)
    causal = jnp.arange(BLK)[:, None] >= jnp.arange(BLK)[None, :]
    local_weight = lax.dynamic_slice_in_dim(mix_weight, group_start, groups_here, 0)
    masked = jnp.where(causal[None], local_weight, jnp.zeros_like(local_weight))
    local_bias = lax.dynamic_slice_in_dim(mix_bias, group_start, groups_here, 0).astype(jnp.float32)
    normed_blocks = normed.reshape(blocks, BLK, groups_here, span_width)
    mixed = jnp.einsum("gts,nsgd->ntgd", masked, normed_blocks, preferred_element_type=jnp.float32)
    mixed = (mixed + local_bias.T[None, :, :, None]).reshape(seq_len, channels)
    gated = (unit_act * mixed).astype(jnp.bfloat16)
    weight_whole = lax.all_gather(out_weight, "dp", axis=0, tiled=True)
    dy_rows = lax.all_gather(cotangent, "sp", axis=1, tiled=True)[0]
    product = jnp.dot(dy_rows, weight_whole, preferred_element_type=jnp.float32)
    weight_part = lax.dot_general(
        dy_rows, gated, (((0,), (0,)), ((), ())), preferred_element_type=jnp.float32
    )
    token_count = lax.axis_size("dp") * seq_len
    norm_scale = 1.0 / math.sqrt(token_count)
    mix_scale = 1.0 / math.sqrt(token_count // BLK * group_dim)
    out_grad = (
        lax.psum_scatter(
            weight_part.astype(jnp.bfloat16), "dp", scatter_dimension=0, tiled=True
        ).astype(jnp.float32)
        * norm_scale
    )
    unit_grad = (product * mixed * gelu_slope(units)).astype(jnp.bfloat16)
    mix_grad = product * unit_act
    mix_round = mix_grad.astype(jnp.bfloat16).reshape(blocks, BLK, groups_here, span_width)
    mix_term = jnp.einsum(
        "ntgd,nsgd->gts", mix_round, normed_blocks, preferred_element_type=jnp.float32
    )
    mix_term = jnp.where(causal[None], mix_term, jnp.float32(0.0))
    bias_term = jnp.sum(mix_grad.reshape(blocks, BLK, groups_here, span_width), axis=(0, 3)).T
    normed_grad = jnp.einsum(
        "gts,ntgd->nsgd", masked, mix_round, preferred_element_type=jnp.float32
    ).reshape(seq_len, channels)
    gain_term = jnp.sum(normed_grad * centred, axis=0)
    shift_term = jnp.sum(normed_grad, axis=0)
    scaled = normed_grad * gain_vec
    back_sums = lax.psum((jnp.sum(scaled, axis=-1), jnp.sum(scaled * centred, axis=-1)), "sp")
    first_m = back_sums[0] / GW
    second_m = back_sums[1] / GW
    gate_grad = (
        rstd_val[:, None]
        * (scaled - first_m[:, None] - centred * second_m[:, None])
        * gelu_slope(gates)
    ).astype(jnp.bfloat16)
    empty_weight = jnp.zeros((GROUPS, BLK, BLK), jnp.float32)
    empty_bias = jnp.zeros((GROUPS, BLK), jnp.float32)
    mix_local, bias_local, gain_total, shift_total = (
        lax.psum(mix_term.astype(jnp.bfloat16), "dp").astype(jnp.float32),
        lax.psum(bias_term.astype(jnp.bfloat16), "dp").astype(jnp.float32),
        lax.psum(gain_term.astype(jnp.bfloat16), "dp").astype(jnp.float32),
        lax.psum(shift_term.astype(jnp.bfloat16), "dp").astype(jnp.float32),
    )
    full_weight = lax.dynamic_update_slice_in_dim(empty_weight, mix_local, group_start, 0)
    full_bias = lax.dynamic_update_slice_in_dim(empty_bias, bias_local, group_start, 0)
    full_weight, full_bias = (
        lax.psum(full_weight.astype(jnp.bfloat16), "sp").astype(jnp.float32),
        lax.psum(full_bias.astype(jnp.bfloat16), "sp").astype(jnp.float32),
    )
    return (
        unit_grad[None],
        gate_grad[None],
        out_grad,
        full_weight * mix_scale,
        full_bias * mix_scale,
        gain_total * norm_scale,
        shift_total * norm_scale,
    )


def solution(mesh):
    in_specs = (
        P("dp", "sp", None),
        P("dp", None, "sp"),
        P("dp", None, "sp"),
        P("dp", "sp"),
        P(),
        P(),
        P("sp"),
        P("sp"),
    )
    out_specs = (
        P("dp", None, "sp"),
        P("dp", None, "sp"),
        P("dp", "sp"),
        P(),
        P(),
        P("sp"),
        P("sp"),
    )
    return jax.shard_map(local, mesh=mesh, in_specs=in_specs, out_specs=out_specs, check_vma=False)
```

profile of v0, /device:TPU:0, one launch (start us, length us, event | category | flops | bytes accessed | tf_op | source)
XLA Modules:
  0.0 237.9 jit_solution(5552104702866696244)
XLA Ops:
  7.2 0.0 all-gather.3.cloned.1.call-start
  7.2 0.7 all-gather.3.cloned.1.call-update
  7.9 0.0 copy-start.5
  7.9 0.0 copy-start.6
  7.9 0.0 copy-start.2
  7.9 0.0 all-gather.5.cloned.1.call-start
  8.0 0.7 all-gather.5.cloned.1.call-update
  8.7 0.0 all-reduce.6.cloned.1.call-start
  8.7 1.7 reshape.181
  10.4 0.5 copy.70
  10.9 0.0 copy-done.5
  11.0 0.0 copy-start
  11.0 0.0 copy-done.6
  11.0 0.0 copy-done.2
  11.0 0.0 copy-start.7
  11.0 0.6 reshape.185
  11.7 1.3 copy.78
  13.0 0.0 copy-done
  13.0 0.5 fusion.70
  13.5 13.9 %all-reduce.1 = (f32[512]{0:T(512)S(1)}, f32[512]{0:T(512)S(1)}) all-reduce(f32[512]{0:T(512)S(1)} %get-tuple-element.40, f32[512]{0:T(512)S(1)} %get-tuple-element.39), channel_id=1, replica_groups=mesh['sp'=4,'dp'=8] {'sp'}, use_global_device_ids=true, to_apply=%region_3.4 | all-reduce | flops 1024 | bytes 8192 | tf_op jit(solution)/shard_map/psum | solution.py:34
  27.5 0.7 convert_bitcast_fusion.1
  28.2 0.0 copy-done.7
  28.2 3.3 %fusion.43 = (bf16[4,128,2,256]{1,3,0,2:T(8,128)(2,1)}, f32[4,128,2,256]{1,3,0,2:T(8,128)}) fusion(f32[4,128,2,256]{1,3,0,2:T(8,128)} %copy.78, f32[128,2]{0,1:T(2,128)S(1)} %convert_bitcast_fusion.1, bf16[8,128,128]{2,1,0:T(8,128)(2,1)S(1)} %copy-done.7, s32[]{:T(128)S(6)} %select_n.20, pred[128,128]{1,0:T(8,128)(4,1)S(1)} %iota_compare_fusion, ...), kind=kOutput, calls=%fused_computation.64 | convolution fusion | flops 73433088 | bytes 3761156 | tf_op jit(solution)/shard_map/gts,nsgd->ntgd/dot_general | solution.py:46
  31.5 1.5 copy.71
  33.0 1.0 copy.87
  34.1 24.0 %all-gather.3.cloned.1.call-done = bf16[1,512,2048]{2,1,0:T(8,128)(2,1)} async-done(((bf16[1,128,2048]{2,1,0:T(8,128)(2,1)}), bf16[1,512,2048]{2,1,0:T(8,128)(2,1)}) %all-gather.3.cloned.1.call-update) | async-done | bytes 2097168 | tf_op jit(solution)/shard_map/all_gather | solution.py:50
  58.0 28.5 %all-gather.5.cloned.1.call-done = bf16[2048,512]{1,0:T(8,128)(2,1)} async-done(((bf16[256,512]{1,0:T(8,128)(2,1)}), bf16[2048,512]{1,0:T(8,128)(2,1)}) %all-gather.5.cloned.1.call-update) | async-done | bytes 2097168 | tf_op jit(solution)/shard_map/all_gather | solution.py:49
  86.6 5.6 %fusion.85 = (bf16[512,512]{1,0:T(8,128)(2,1)}, f32[512,512]{1,0:T(8,128)S(1)}, bf16[1,512,512]{2,1,0:T(8,128)(2,1)}) fusion(bf16[1,512,512]{2,1,0:T(8,128)(2,1)S(1)} %copy-done.2, f32[512,512]{1,0:T(8,128)} %bitcast.107, bf16[2048,512]{1,0:T(8,128)(2,1)} %all-gather.5.cloned.1.call-done, bf16[1,512,2048]{2,1,0:T(8,128)(2,1)} %all-gather.3.cloned.1.call-done), kind=kOutput, calls=%fused_computation.126 | convolution fusion | flops 1081868288 | bytes 7864320 | tf_op jit(solution)/shard_map/dot_general | solution.py:51
  92.2 1.2 reshape.178
  93.3 0.0 copy-start.3
  93.3 1.4 fusion.10
  94.7 0.0 copy-done.3
  94.7 0.0 all-reduce.6.cloned.1.call-update
  94.7 0.0 all-reduce.8.cloned.1.call-start
  94.8 1.4 copy.79
  96.2 0.9 copy.88
  97.1 51.0 %all-reduce.6.cloned.1.call-done = bf16[2,128,128]{2,1,0:T(8,128)(2,1)} async-done(((bf16[2,128,128]{2,1,0:T(8,128)(2,1)}), bf16[2,128,128]{2,1,0:T(8,128)(2,1)}) %all-reduce.6.cloned.1.call-update) | async-done | bytes 65552 | tf_op jit(solution)/shard_map/psum | solution.py:89
  148.1 0.9 convert_dynamic-update-slice_fusion
  149.0 0.0 copy-start.1
  149.0 0.7 copy-done.1
  149.7 0.0 all-reduce.8.cloned.1.call-update
  149.7 0.0 reduce-scatter.2.cloned.1.call-start
  149.7 4.3 %fusion = bf16[2048,512]{0,1:T(8,128)(2,1)} fusion(bf16[512,512]{1,0:T(8,128)(2,1)} %bitcast.108, bf16[1,512,2048]{2,1,0:T(8,128)(2,1)} %all-gather.3.cloned.1.call-done), kind=kOutput, calls=%fused_computation.13 | convolution fusion | flops 1074790400 | bytes 4718592 | tf_op jit(solution)/shard_map/dot_general | solution.py:52
  154.1 0.0 copy-start.4
  154.1 0.0 reduce-scatter.2.cloned.1.call-update
  154.1 1.0 copy-done.4
  155.1 1.8 multiply_reduce_fusion
  156.9 0.7 reshape.180
  157.6 0.4 reduce_sum.73
  158.0 0.1 copy.91
  158.1 1.6 copy.73
  159.6 0.8 reshape.179
  160.5 11.8 %all-reduce.2 = (bf16[2,128]{1,0:T(2,128)(2,1)S(1)}, bf16[512]{0:T(512)(128)(2,1)S(1)}, bf16[512]{0:T(512)(128)(2,1)S(1)}) all-reduce(bf16[2,128]{1,0:T(2,128)(2,1)S(1)} %bitcast.114, bf16[512]{0:T(512)(128)(2,1)S(1)} %bitcast.112, bf16[512]{0:T(512)(128)(2,1)S(1)} %bitcast.113), channel_id=1, replica_groups=mesh['sp'=4,'dp'=8] {'dp'}, use_global_device_ids=true, to_apply=%region_12.13 | all-reduce | flops 1280 | bytes 5120 | tf_op jit(solution)/shard_map/psum | solution.py:90
  172.3 0.1 dynamic_update_slice.7
  172.4 12.0 %psum.77 = bf16[8,128]{1,0:T(8,128)(2,1)S(1)} all-reduce(bf16[8,128]{1,0:T(8,128)(2,1)S(1)} %dynamic_update_slice.7), channel_id=1, replica_groups=mesh['sp'=4,'dp'=8] {'sp'}, use_global_device_ids=true, to_apply=%region_13.14 | all-reduce | flops 1024 | bytes 4096 | tf_op jit(solution)/shard_map/psum | solution.py:98
  184.4 8.4 %all-reduce = (f32[512]{0:T(512)S(1)}, f32[512]{0:T(512)S(1)}) all-reduce(f32[512]{0:T(512)S(1)} %bitcast.115, f32[512]{0:T(512)S(1)} %bitcast.116), channel_id=1, replica_groups=mesh['sp'=4,'dp'=8] {'sp'}, use_global_device_ids=true, to_apply=%region_7.8 | all-reduce | flops 1024 | bytes 8192 | tf_op jit(solution)/shard_map/psum | solution.py:78
  192.7 0.6 convert_multiply_fusion.11
  193.3 0.6 convert_multiply_fusion.12
  193.9 2.1 fusion.69
  196.1 0.0 all-reduce.8.cloned.1.call-done
  196.1 1.8 convert_multiply_fusion.9
  197.9 31.5 %reduce-scatter.2.cloned.1.call-done = bf16[256,512]{0,1:T(8,128)(2,1)} async-done(((bf16[2048,512]{0,1:T(8,128)(2,1)}), bf16[256,512]{0,1:T(8,128)(2,1)}) %reduce-scatter.2.cloned.1.call-update) | async-done | bytes 262160 | tf_op jit(solution)/shard_map/reduce_scatter | solution.py:59
  229.4 1.0 convert_multiply_fusion.10
  230.4 1.0 copy.83
  (10 shorter events, 0.1 us)
Async XLA Ops:
  7.2 50.9 %all-gather.3.cloned.1.call-start = ((), (), s32[]{:S(2)}) async-start(), calls=%async_computation.1 | async-start | bytes 2621440 | tf_op jit(solution)/shard_map/all_gather | solution.py:50
  7.9 3.0 %copy-start.5 = (bf16[512]{0:T(512)(128)(2,1)S(1)}, bf16[512]{0:T(512)(128)(2,1)}, u32[]{:S(2)}) copy-start(bf16[512]{0:T(512)(128)(2,1)} %param.14) | copy-start | bytes 3076
  7.9 3.1 %copy-start.6 = (bf16[512]{0:T(512)(128)(2,1)S(1)}, bf16[512]{0:T(512)(128)(2,1)}, u32[]{:S(2)}) copy-start(bf16[512]{0:T(512)(128)(2,1)} %param.15) | copy-start | bytes 3076
  7.9 3.1 %copy-start.2 = (bf16[1,512,512]{2,1,0:T(8,128)(2,1)S(1)}, bf16[1,512,512]{2,1,0:T(8,128)(2,1)}, u32[]{:S(2)}) copy-start(bf16[1,512,512]{2,1,0:T(8,128)(2,1)} %param.9) | copy-start | bytes 1572868
  7.9 78.7 %all-gather.5.cloned.1.call-start = ((), (), s32[]{:S(2)}) async-start(), calls=%async_computation.2 | async-start | bytes 2359296 | tf_op jit(solution)/shard_map/all_gather | solution.py:49
  8.7 139.4 %all-reduce.6.cloned.1.call-start = ((), (), s32[]{:S(2)}) async-start(), calls=%async_computation.4 | async-start | bytes 131072 | tf_op jit(solution)/shard_map/psum | solution.py:89
  11.0 2.0 copy-start
  11.0 17.2 %copy-start.7 = (bf16[8,128,128]{2,1,0:T(8,128)(2,1)S(1)}, bf16[8,128,128]{2,1,0:T(8,128)(2,1)}, u32[]{:S(2)}) copy-start(bf16[8,128,128]{2,1,0:T(8,128)(2,1)} %param.12) | copy-start | bytes 786436
  93.3 1.4 copy-start.3
  94.7 101.3 %all-reduce.8.cloned.1.call-start = ((), (), s32[]{:S(2)}) async-start(), calls=%async_computation.5 | async-start | bytes 524288 | tf_op jit(solution)/shard_map/psum | solution.py:97
  149.0 0.7 copy-start.1
  149.7 79.7 %reduce-scatter.2.cloned.1.call-start = ((), (), s32[]{:S(2)}) async-start(), calls=%async_computation.3 | async-start | bytes 2359296 | tf_op jit(solution)/shard_map/reduce_scatter | solution.py:59
  154.1 1.1 copy-start.4
Sparse Core Ops, SparseCore 0:
  9.5 48.4 all-gather.2
  59.9 26.6 all-gather.4
  94.9 53.1 all-reduce.5
  150.3 35.0 all-reduce.7
  188.4 40.9 reduce-scatter.1
where the time goes:
time: 238 us
  waiting for transfers between devices  136 us (57%)
  blocking collectives  46.1 us (19%)
  matrix products  16.3 us (7%)
  local copies, waits for them, and re-layouts  16.2 us (7%)
  between operations  14 us (6%)
  other arithmetic  8.61 us (4%)
    psum x1, waiting for transfers between devices, local(): lax.psum(mix_term.astype(jnp.bfloat16), 'dp').astype(jnp.float32)  51 us
    reduce_scatter x1, waiting for transfers between devices, local(): lax.psum_scatter(weight_part.astype(jnp.bfloat16), 'dp', scatter_dimensio...  31.5 us
    all_gather x1, waiting for transfers between devices, local(): weight_whole = lax.all_gather(out_weight, 'dp', axis=0, tiled=True)  28.5 us
    all_gather x1, waiting for transfers between devices, local(): dy_rows = lax.all_gather(cotangent, 'sp', axis=1, tiled=True)[0]  24 us
    psum x1, blocking collectives, local(): lax.psum((jnp.sum(gate_act, axis=-1), jnp.sum(gate_act * gate_act, axis=-...  13.9 us
    psum x1, blocking collectives, local(): lax.psum(full_bias.astype(jnp.bfloat16), 'sp').astype(jnp.float32)  12 us
    psum x1, blocking collectives, local(): lax.psum(bias_term.astype(jnp.bfloat16), 'dp').astype(jnp.float32)  11.8 us
    psum x1, blocking collectives, local(): lax.psum((jnp.sum(scaled, axis=-1), jnp.sum(scaled * centred, axis=-1)),...  8.36 us
  transfers between devices with their start and end apart: 5, of which 4 were waited for; matrix products, arithmetic and copies ran while one was open for 12% of the time, Pallas kernels for 0%

commit v1 on v0

--- a/solution.py
+++ b/solution.py
@@ -86,7 +86,7 @@
     empty_weight = jnp.zeros((GROUPS, BLK, BLK), jnp.float32)
     empty_bias = jnp.zeros((GROUPS, BLK), jnp.float32)
     mix_local, bias_local, gain_total, shift_total = (
-        lax.psum(mix_term.astype(jnp.bfloat16), "dp").astype(jnp.float32),
+        jnp.sum(lax.all_gather(mix_term.astype(jnp.bfloat16), "dp"), axis=0).astype(jnp.float32),
         lax.psum(bias_term.astype(jnp.bfloat16), "dp").astype(jnp.float32),
         lax.psum(gain_term.astype(jnp.bfloat16), "dp").astype(jnp.float32),
         lax.psum(shift_term.astype(jnp.bfloat16), "dp").astype(jnp.float32),

time: 238 us -> 195 us (0.82)
  waiting for transfers between devices: 136 us -> 82.2 us
  blocking collectives: 46.1 us -> 57 us
    psum x1 -> x0, waiting for transfers between devices: 51 us -> none  [local(): lax.psum(mix_term.astype(jnp.bfloat16), 'dp').astype(jnp.float32)]
    all_gather x0 -> x1, blocking collectives: none -> 9.82 us  [local(): lax.all_gather(mix_term.astype(jnp.bfloat16), 'dp')]
  transfers between devices with their start and end apart: 5 -> 4, of which waited for: 4 -> 3; matrix products, arithmetic and copies ran while one was open for 12% -> 15% of each run, Pallas kernels for 0% -> 0%
where the time goes in v1:
time: 195 us; the launch traced here: 194 us
  waiting for transfers between devices  82.2 us (42%)
  blocking collectives  57 us (29%)
  local copies, waits for them, and re-layouts  17 us (9%)
  matrix products  15.7 us (8%)
  between operations  14 us (7%)
  other arithmetic  7.81 us (4%)
    reduce_scatter x1, waiting for transfers between devices, local(): lax.psum_scatter(weight_part.astype(jnp.bfloat16), 'dp', scatter_dimensio...  30.5 us
    all_gather x1, waiting for transfers between devices, local(): weight_whole = lax.all_gather(out_weight, 'dp', axis=0, tiled=True)  28.5 us
    all_gather x1, waiting for transfers between devices, local(): dy_rows = lax.all_gather(cotangent, 'sp', axis=1, tiled=True)[0]  21.7 us
    psum x1, blocking collectives, local(): lax.psum((jnp.sum(gate_act, axis=-1), jnp.sum(gate_act * gate_act, axis=-...  13.9 us
    psum x1, blocking collectives, local(): lax.psum(bias_term.astype(jnp.bfloat16), 'dp').astype(jnp.float32)  13.6 us
    psum x1, blocking collectives, local(): lax.psum(full_bias.astype(jnp.bfloat16), 'sp').astype(jnp.float32)  11.3 us
    all_gather x1, blocking collectives, local(): lax.all_gather(mix_term.astype(jnp.bfloat16), 'dp')  9.82 us
    psum x1, blocking collectives, local(): lax.psum((jnp.sum(scaled, axis=-1), jnp.sum(scaled * centred, axis=-1)),...  8.39 us
  transfers between devices with their start and end apart: 4, of which 3 were waited for; matrix products, arithmetic and copies ran while one was open for 15% of the time, Pallas kernels for 0%

profile of v1, /device:TPU:0, one launch (start us, length us, event | category | flops | bytes accessed | tf_op | source)
XLA Modules:
  0.0 194.1 jit_solution(13900895700849009858)
XLA Ops:
  7.2 0.0 all-gather.4.cloned.1.call-start
  7.2 0.7 all-gather.4.cloned.1.call-update
  7.9 0.0 copy-start.5
  7.9 0.0 copy-start.6
  7.9 0.0 copy-start.2
  7.9 0.0 all-gather.6.cloned.1.call-start
  8.0 0.7 all-gather.6.cloned.1.call-update
  8.7 0.0 all-reduce.5.cloned.1.call-start
  8.7 1.7 reshape.181
  10.4 0.5 copy.70
  10.9 0.0 copy-done.5
  11.0 0.0 copy-start
  11.0 0.0 copy-done.6
  11.0 0.0 copy-done.2
  11.0 0.0 copy-start.7
  11.0 0.6 reshape.185
  11.7 1.3 copy.78
  13.0 0.0 copy-done
  13.0 0.5 fusion.70
  13.5 13.9 %all-reduce.1 = (f32[512]{0:T(512)S(1)}, f32[512]{0:T(512)S(1)}) all-reduce(f32[512]{0:T(512)S(1)} %get-tuple-element.40, f32[512]{0:T(512)S(1)} %get-tuple-element.39), channel_id=1, replica_groups=mesh['sp'=4,'dp'=8] {'sp'}, use_global_device_ids=true, to_apply=%region_3.4 | all-reduce | flops 1024 | bytes 8192 | tf_op jit(solution)/shard_map/psum | solution.py:34
  27.5 0.7 convert_bitcast_fusion.1
  28.2 0.0 copy-done.7
  28.2 3.3 %fusion.43 = (bf16[4,128,2,256]{1,3,0,2:T(8,128)(2,1)}, f32[4,128,2,256]{1,3,0,2:T(8,128)}) fusion(f32[4,128,2,256]{1,3,0,2:T(8,128)} %copy.78, f32[128,2]{0,1:T(2,128)S(1)} %convert_bitcast_fusion.1, bf16[8,128,128]{2,1,0:T(8,128)(2,1)S(1)} %copy-done.7, s32[]{:T(128)S(6)} %select_n.20, pred[128,128]{1,0:T(8,128)(4,1)S(1)} %iota_compare_fusion, ...), kind=kOutput, calls=%fused_computation.64 | convolution fusion | flops 73433088 | bytes 3761156 | tf_op jit(solution)/shard_map/gts,nsgd->ntgd/dot_general | solution.py:46
  31.5 1.5 copy.71
  33.0 1.0 copy.87
  34.1 1.4 copy.79
  35.5 0.9 copy.88
  36.3 21.7 %all-gather.4.cloned.1.call-done = bf16[1,512,2048]{2,1,0:T(8,128)(2,1)} async-done(((bf16[1,128,2048]{2,1,0:T(8,128)(2,1)}), bf16[1,512,2048]{2,1,0:T(8,128)(2,1)}) %all-gather.4.cloned.1.call-update) | async-done | bytes 2097168 | tf_op jit(solution)/shard_map/all_gather | solution.py:50
  58.0 28.5 %all-gather.6.cloned.1.call-done = bf16[2048,512]{1,0:T(8,128)(2,1)} async-done(((bf16[256,512]{1,0:T(8,128)(2,1)}), bf16[2048,512]{1,0:T(8,128)(2,1)}) %all-gather.6.cloned.1.call-update) | async-done | bytes 2097168 | tf_op jit(solution)/shard_map/all_gather | solution.py:49
  86.6 5.6 %fusion.85 = (bf16[512,512]{1,0:T(8,128)(2,1)}, f32[512,512]{1,0:T(8,128)S(1)}, bf16[1,512,512]{2,1,0:T(8,128)(2,1)}) fusion(bf16[1,512,512]{2,1,0:T(8,128)(2,1)S(1)} %copy-done.2, f32[512,512]{1,0:T(8,128)} %bitcast.109, bf16[2048,512]{1,0:T(8,128)(2,1)} %all-gather.6.cloned.1.call-done, bf16[1,512,2048]{2,1,0:T(8,128)(2,1)} %all-gather.4.cloned.1.call-done), kind=kOutput, calls=%fused_computation.126 | convolution fusion | flops 1081868288 | bytes 7864320 | tf_op jit(solution)/shard_map/dot_general | solution.py:51
  92.2 1.2 reshape.178
  93.3 0.0 copy-start.3
  93.3 0.8 copy-done.3
  94.1 0.7 fusion.10
  94.9 9.8 %all-gather = bf16[16,128,128]{2,1,0:T(8,128)(2,1)S(1)} all-gather(bf16[2,128,128]{2,1,0:T(8,128)(2,1)S(1)} %fusion.10), channel_id=2, replica_groups=mesh['sp'=4,'dp'=8] {'dp'}, dimensions={0}, use_global_device_ids=true | all-gather | bytes 589824 | tf_op jit(solution)/shard_map/all_gather | solution.py:89
  104.7 0.1 reduce_sum.85
  104.8 0.0 copy-start.1
  104.8 0.7 copy-done.1
  105.5 0.0 all-reduce.5.cloned.1.call-update
  105.6 0.2 reduce-scatter.2.cloned.1.call-start
  105.8 4.3 %fusion = bf16[2048,512]{0,1:T(8,128)(2,1)} fusion(bf16[512,512]{1,0:T(8,128)(2,1)} %bitcast.110, bf16[1,512,2048]{2,1,0:T(8,128)(2,1)} %all-gather.4.cloned.1.call-done), kind=kOutput, calls=%fused_computation.13 | convolution fusion | flops 1074790400 | bytes 4718592 | tf_op jit(solution)/shard_map/dot_general | solution.py:52
  110.1 0.0 copy-start.4
  110.1 0.0 reduce-scatter.2.cloned.1.call-update
  110.2 1.0 copy-done.4
  111.2 1.8 multiply_reduce_fusion
  113.0 0.7 reshape.180
  113.6 0.4 reduce_sum.86
  114.0 0.1 copy.91
  114.1 1.6 copy.73
  115.7 0.8 reshape.179
  116.5 13.6 %all-reduce.2 = (bf16[2,128]{1,0:T(2,128)(2,1)S(1)}, bf16[512]{0:T(512)(128)(2,1)S(1)}, bf16[512]{0:T(512)(128)(2,1)S(1)}) all-reduce(bf16[2,128]{1,0:T(2,128)(2,1)S(1)} %bitcast.116, bf16[512]{0:T(512)(128)(2,1)S(1)} %bitcast.114, bf16[512]{0:T(512)(128)(2,1)S(1)} %bitcast.115), channel_id=1, replica_groups=mesh['sp'=4,'dp'=8] {'dp'}, use_global_device_ids=true, to_apply=%region_12.13 | all-reduce | flops 1280 | bytes 5120 | tf_op jit(solution)/shard_map/psum | solution.py:90
  130.1 0.1 dynamic_update_slice.7
  130.2 11.3 %psum.69 = bf16[8,128]{1,0:T(8,128)(2,1)S(1)} all-reduce(bf16[8,128]{1,0:T(8,128)(2,1)S(1)} %dynamic_update_slice.7), channel_id=1, replica_groups=mesh['sp'=4,'dp'=8] {'sp'}, use_global_device_ids=true, to_apply=%region_13.14 | all-reduce | flops 1024 | bytes 4096 | tf_op jit(solution)/shard_map/psum | solution.py:98
  141.5 8.4 %all-reduce = (f32[512]{0:T(512)S(1)}, f32[512]{0:T(512)S(1)}) all-reduce(f32[512]{0:T(512)S(1)} %bitcast.117, f32[512]{0:T(512)S(1)} %bitcast.118), channel_id=1, replica_groups=mesh['sp'=4,'dp'=8] {'sp'}, use_global_device_ids=true, to_apply=%region_7.8 | all-reduce | flops 1024 | bytes 8192 | tf_op jit(solution)/shard_map/psum | solution.py:78
  149.9 0.6 convert_multiply_fusion.11
  150.5 0.6 convert_multiply_fusion.12
  151.1 2.1 %fusion.69 = bf16[1,512,512]{2,1,0:T(8,128)(2,1)} fusion(bf16[1,512,512]{2,1,0:T(8,128)(2,1)S(1)} %copy-done, f32[1,512,512]{2,1,0:T(8,128)S(1)} %reshape.179, f32[512]{0:T(512)S(1)} %get-tuple-element.57, f32[512]{0:T(512)S(1)} %get-tuple-element.51, f32[512]{0:T(512)S(1)} %get-tuple-element.58, f32[512]{0:T(512)S(1)} %convert_element_type.114, ...), kind=kLoop, calls=%fused_computation.95 | loop fusion | flops 9175040 | bytes 2107392 | tf_op jit(solution)/shard_map/convert_element_type | solution.py:85
  153.2 0.0 all-reduce.5.cloned.1.call-done
  153.2 1.8 convert_multiply_fusion.9
  155.0 30.5 %reduce-scatter.2.cloned.1.call-done = bf16[256,512]{0,1:T(8,128)(2,1)} async-done(((bf16[2048,512]{0,1:T(8,128)(2,1)}), bf16[256,512]{0,1:T(8,128)(2,1)}) %reduce-scatter.2.cloned.1.call-update) | async-done | bytes 262160 | tf_op jit(solution)/shard_map/reduce_scatter | solution.py:59
  185.6 1.0 convert_multiply_fusion.10
  186.5 1.0 copy.83
  (11 shorter events, 0.1 us)
Async XLA Ops:
  7.2 50.9 %all-gather.4.cloned.1.call-start = ((), (), s32[]{:S(2)}) async-start(), calls=%async_computation.1 | async-start | bytes 2621440 | tf_op jit(solution)/shard_map/all_gather | solution.py:50
  7.9 3.0 %copy-start.5 = (bf16[512]{0:T(512)(128)(2,1)S(1)}, bf16[512]{0:T(512)(128)(2,1)}, u32[]{:S(2)}) copy-start(bf16[512]{0:T(512)(128)(2,1)} %param.14) | copy-start | bytes 3076
  7.9 3.1 %copy-start.6 = (bf16[512]{0:T(512)(128)(2,1)S(1)}, bf16[512]{0:T(512)(128)(2,1)}, u32[]{:S(2)}) copy-start(bf16[512]{0:T(512)(128)(2,1)} %param.15) | copy-start | bytes 3076
  7.9 3.1 %copy-start.2 = (bf16[1,512,512]{2,1,0:T(8,128)(2,1)S(1)}, bf16[1,512,512]{2,1,0:T(8,128)(2,1)}, u32[]{:S(2)}) copy-start(bf16[1,512,512]{2,1,0:T(8,128)(2,1)} %param.9) | copy-start | bytes 1572868
  7.9 78.7 %all-gather.6.cloned.1.call-start = ((), (), s32[]{:S(2)}) async-start(), calls=%async_computation.2 | async-start | bytes 2359296 | tf_op jit(solution)/shard_map/all_gather | solution.py:49
  8.7 144.6 %all-reduce.5.cloned.1.call-start = ((), (), s32[]{:S(2)}) async-start(), calls=%async_computation.4 | async-start | bytes 524288 | tf_op jit(solution)/shard_map/psum | solution.py:97
  11.0 2.0 %copy-start = (bf16[1,512,512]{2,1,0:T(8,128)(2,1)S(1)}, bf16[1,512,512]{2,1,0:T(8,128)(2,1)}, u32[]{:S(2)}) copy-start(bf16[1,512,512]{2,1,0:T(8,128)(2,1)} %param.10) | copy-start | bytes 1572868
  11.0 17.2 %copy-start.7 = (bf16[8,128,128]{2,1,0:T(8,128)(2,1)S(1)}, bf16[8,128,128]{2,1,0:T(8,128)(2,1)}, u32[]{:S(2)}) copy-start(bf16[8,128,128]{2,1,0:T(8,128)(2,1)} %param.12) | copy-start | bytes 786436
  93.3 0.8 copy-start.3
  104.8 0.7 copy-start.1
  105.6 80.0 %reduce-scatter.2.cloned.1.call-start = ((), (), s32[]{:S(2)}) async-start(), calls=%async_computation.3 | async-start | bytes 2359296 | tf_op jit(solution)/shard_map/reduce_scatter | solution.py:59
  110.1 1.1 copy-start.4
Sparse Core Ops, SparseCore 0:
  9.5 48.4 all-gather.3
  59.9 26.6 all-gather.5
  105.7 35.6 all-reduce.4
  144.5 40.9 reduce-scatter.1
